TPU v7x, 32 devices: a whole 2x2x4 slice. The times are simulated.
32 devices in a mesh: ep: 32 (over z, y, x, core).
Axes of the slice: x: 2, y: 2, z: 4, core: 2. Of those that a mesh axis runs over, the one named last changes fastest.
Arguments:
- residual_in: bfloat16 [256, 2048], P('ep'), may hold values from -6 to 6
- gain_mix_pre: float32 [2048], replicated, may hold values from 0.1 to 1.9
- w_query: bfloat16 [2048, 2048], P(None, 'ep'), may hold values from -0.125 to 0.125
- w_key: bfloat16 [2048, 2048], P(None, 'ep'), may hold values from -0.125 to 0.125
- w_value: bfloat16 [2048, 2048], P(None, 'ep'), may hold values from -0.125 to 0.125
- w_outgate: bfloat16 [2048, 2048], P(None, 'ep'), may hold values from -0.125 to 0.125
- w_decay: bfloat16 [2048, 16], replicated, may hold values from -0.125 to 0.125
- w_beta: bfloat16 [2048, 16], replicated, may hold values from -0.125 to 0.125
- decay_scale: float32 [16], replicated, may hold values from 1 to 16
- decay_bias: float32 [16], replicated, may hold values from -5 to -1
- head_gain: float32 [128], replicated, may hold values from 0.1 to 1.9
- w_out: bfloat16 [2048, 2048], replicated, may hold values from -0.125 to 0.125
- gain_mix_post: float32 [2048], replicated, may hold values from 0.1 to 1.9
- state_cache: bfloat16 [256, 16, 128, 128], P('ep'), may hold values from -2.390625 to 2.390625
- gain_ffn_pre: float32 [2048], replicated, may hold values from 0.1 to 1.9
- routes: int32 [256, 4], P('ep'), may hold values from 0 to 7, all different within a row; in each aligned block of 8 rows (0 to 7, 8 to 15, ...) at most 8 rows name the same one
- route_logits: float32 [256, 4], P('ep'), may hold values from -6 to 6
- w_gate: bfloat16 [2048, 16384], P(None, 'ep'), may hold values from -0.375 to 0.375
- w_up: bfloat16 [2048, 16384], P(None, 'ep'), may hold values from -0.375 to 0.375
- w_down: bfloat16 [16384, 2048], P('ep'), may hold values from -0.125 to 0.125
- gain_ffn_post: float32 [2048], replicated, may hold values from 0.1 to 1.9
Outputs:
- result: bfloat16 [256, 2048], P('ep')
- new_state: bfloat16 [256, 16, 128, 128], P('ep')
Inputs may be any that keep to these rules, and one draw needn't show every extreme that they name: `routes`: each row names 4 different experts. In the rows of one device (aligned blocks of 8 rows) no expert is named more than 8 times, and in some block one expert is named exactly 8 times.
All inputs are finite; a program needn't handle non-finite values.
Results may differ from a plain program's by a relative error of at most 0.014.
Values may be sent and summed in bfloat16 or wider, within the bound.
A program may use at most 128 MiB of HBM per device.

v0:
```python
import jax
import jax.numpy as jnp
from jax import lax
from jax.sharding import PartitionSpec as P

H = 16
HD = 128
PIECES = 4
TOPK = 4


EPS = 1e-06
LIMIT = 7.0
ALPHA = 1.702


def rms_scale(values):
    return values * lax.rsqrt(jnp.mean(values * values, axis=-1, keepdims=True) + EPS)


def clamped_unit(gate, upper):
    glu = jnp.minimum(gate, LIMIT)
    linear = jnp.clip(upper, -LIMIT, LIMIT)
    return glu * jax.nn.sigmoid(ALPHA * glu) * (linear + 1.0)


def dispatch_table(routes, experts, capacity):
    count, topk = routes.shape
    hits = (routes[:, :, None] == jnp.arange(experts, dtype=jnp.int32)).astype(jnp.int32)
    flat = hits.reshape(count * topk, experts)
    before = jnp.cumsum(flat, axis=0) - flat
    slots = jnp.sum(before * flat, axis=1).reshape(count, topk)
    target = routes * capacity + slots
    return (target[:, :, None] == jnp.arange(experts * capacity, dtype=jnp.int32)).astype(
        jnp.float32
    )


def delta_step(
    q_raw, k_raw, v_raw, z_raw, decay_in, beta_in, state, decay_scale, decay_bias, head_gain
):
    count = q_raw.shape[0]
    query = jax.nn.silu(q_raw.astype(jnp.float32)).reshape(count, H, HD)
    query = query * lax.rsqrt(jnp.sum(query * query, axis=-1, keepdims=True) + EPS) * HD ** (-0.5)
    keys = jax.nn.silu(k_raw.astype(jnp.float32)).reshape(count, H, HD)
    keys = keys * lax.rsqrt(jnp.sum(keys * keys, axis=-1, keepdims=True) + EPS)
    values = jax.nn.silu(v_raw.astype(jnp.float32)).reshape(count, H, HD)
    decay = -decay_scale * jax.nn.softplus(decay_in + decay_bias)
    beta = jax.nn.sigmoid(beta_in)
    held = state.astype(jnp.float32) * jnp.exp(decay)[:, :, None, None]
    guess = jnp.einsum("rhk,rhkv->rhv", keys, held)
    held = held + jnp.einsum("rhk,rhv->rhkv", keys, beta[:, :, None] * (values - guess))
    output = jnp.einsum("rhk,rhkv->rhv", query, held)
    output = rms_scale(output) * head_gain
    gated = output.reshape(count, H * HD) * jax.nn.silu(z_raw.astype(jnp.float32))
    return (gated.astype(jnp.bfloat16), held.astype(jnp.bfloat16))


def shards(
    residual_in,
    gain_mix_pre,
    w_query,
    w_key,
    w_value,
    w_outgate,
    w_decay,
    w_beta,
    decay_scale,
    decay_bias,
    head_gain,
    w_out,
    gain_mix_post,
    state_cache,
    gain_ffn_pre,
    routes,
    route_logits,
    w_gate,
    w_up,
    w_down,
    gain_ffn_post,
):
    devices = lax.axis_size("ep")
    count, width = residual_in.shape
    x_first = residual_in.astype(jnp.float32)
    normed = (rms_scale(x_first) * gain_mix_pre).astype(jnp.bfloat16)
    stacked = jnp.stack([w_query, w_key, w_value, w_outgate])
    columns = jnp.einsum(
        "td,rdc->trc",
        lax.all_gather(normed, "ep", axis=0, tiled=True),
        stacked,
        preferred_element_type=jnp.float32,
    ).astype(jnp.bfloat16)
    joined = lax.all_to_all(columns, "ep", split_axis=0, concat_axis=2, tiled=True)
    decay_in = jnp.dot(normed, w_decay, preferred_element_type=jnp.float32)
    beta_in = jnp.dot(normed, w_beta, preferred_element_type=jnp.float32)
    mixed, new_state = delta_step(
        joined[:, 0],
        joined[:, 1],
        joined[:, 2],
        joined[:, 3],
        decay_in,
        beta_in,
        state_cache,
        decay_scale,
        decay_bias,
        head_gain,
    )
    branch = jnp.dot(mixed, w_out, preferred_element_type=jnp.float32)
    x_second = x_first + rms_scale(branch) * gain_mix_post
    normed_two = (rms_scale(x_second) * gain_ffn_pre).astype(jnp.bfloat16)
    experts = devices // PIECES
    capacity = max(2, 2 * count * TOPK // experts)
    table = dispatch_table(routes, experts, capacity)
    picks = jnp.sum(table, axis=1).astype(jnp.bfloat16)
    sent = lax.dot_general(
        picks, normed_two, (((0,), (0,)), ((), ())), preferred_element_type=jnp.float32
    ).astype(jnp.bfloat16)
    sent = jnp.broadcast_to(
        sent.reshape(experts, 1, capacity, width), (experts, PIECES, capacity, width)
    ).reshape(devices, capacity, width)
    block = lax.all_to_all(sent, "ep", split_axis=0, concat_axis=0, tiled=True)
    flat = block.reshape(-1, width)
    hidden = clamped_unit(
        jnp.dot(flat, w_gate, preferred_element_type=jnp.float32),
        jnp.dot(flat, w_up, preferred_element_type=jnp.float32),
    ).astype(jnp.bfloat16)
    partial_value = jnp.dot(hidden, w_down, preferred_element_type=jnp.float32).astype(jnp.bfloat16)
    returned = lax.all_to_all(
        partial_value.reshape(block.shape), "ep", split_axis=0, concat_axis=0, tiled=True
    )
    summed = jnp.sum(returned.reshape(experts, PIECES, capacity, width).astype(jnp.float32), axis=1)
    summed = summed.reshape(experts * capacity, width)
    raised = jnp.exp(route_logits)
    weights = raised / jnp.sum(raised, axis=-1, keepdims=True)
    mix_table = jnp.einsum("ske,sk->se", table, weights)
    moe = jnp.dot(mix_table, summed, precision=lax.Precision.HIGHEST)
    result = (x_second + rms_scale(moe) * gain_ffn_post).astype(jnp.bfloat16)
    return (result, new_state)


def solution(mesh):
    in_specs = (
        P("ep", None),
        P(),
        P(None, "ep"),
        P(None, "ep"),
        P(None, "ep"),
        P(None, "ep"),
        P(),
        P(),
        P(),
        P(),
        P(),
        P(),
        P(),
        P("ep", None, None, None),
        P(),
        P("ep", None),
        P("ep", None),
        P(None, "ep"),
        P(None, "ep"),
        P("ep", None),
        P(),
    )
    out_specs = (P("ep", None), P("ep", None, None, None))
    return jax.shard_map(shards, mesh=mesh, in_specs=in_specs, out_specs=out_specs, check_vma=False)
```

profile of v0, /device:TPU:0, one launch (start us, length us, event | category | flops | bytes accessed | tf_op | source)
XLA Modules:
  0.0 168.3 jit_solution(14021566374956665461)
XLA Ops:
  7.2 0.0 copy-start
  7.2 0.0 all-gather.2.cloned.1.call-start
  7.2 1.0 fusion.46
  8.3 1.5 fusion.48
  9.7 0.0 all-gather.2.cloned.1.call-update
  9.7 0.8 copy.47
  10.5 0.1 eq.29
  10.6 0.1 fusion.61
  10.7 0.1 reduce_window_sum.11
  10.7 0.2 select_reduce_fusion
  10.9 0.1 reshape.109
  11.0 0.1 copy.49
  11.1 1.0 fusion.14
  12.1 1.3 pad_maximum_fusion
  13.4 54.4 %all-gather.2.cloned.1.call-done = bf16[256,2048]{1,0:T(8,128)(2,1)} async-done(((bf16[8,2048]{1,0:T(8,128)(2,1)}), bf16[256,2048]{1,0:T(8,128)(2,1)}) %all-gather.2.cloned.1.call-update) | async-done | bytes 1048592 | tf_op jit(solution)/shard_map/all_gather | solution.py:89
  67.8 1.7 %fusion.73 = f32[256,256]{0,1:S(1)} fusion(bf16[256,2048]{1,0:T(8,128)(2,1)} %all-gather.2.cloned.1.call-done, bf16[2048,256]{0,1:T(8,128)(2,1)S(1)} %bitcast.115), kind=kOutput, calls=%fused_computation.122 | convolution fusion | flops 268435456 | bytes 2359296
  69.5 0.0 copy-start.6
  69.5 0.2 copy.41
  69.7 0.8 reshape.127
  70.5 3.6 %all-to-all-start = ((bf16[32,2,1024]{2,1,0:T(2,128)(2,1)}), bf16[32,2,1024]{2,1,0:T(2,128)(2,1)S(1)}, u32[]{:S(2)}, u32[]{:S(2)}) async-start(bf16[32,2,1024]{2,1,0:T(2,128)(2,1)} %reshape.127), calls=%async_computation | async-start | bytes 262144 | tf_op jit(solution)/shard_map/all_to_all | solution.py:93
  74.1 0.1 convert_reduce_fusion.1
  74.2 0.7 neg.38
  74.9 0.1 copy.45
  74.9 1.0 fusion.65
  75.9 6.4 %all-to-all-done = bf16[32,2,1024]{2,1,0:T(2,128)(2,1)S(1)} async-done(((bf16[32,2,1024]{2,1,0:T(2,128)(2,1)}), bf16[32,2,1024]{2,1,0:T(2,128)(2,1)S(1)}, u32[]{:S(2)}, u32[]{:S(2)}) %all-to-all-start) | async-done | bytes 131104 | tf_op jit(solution)/shard_map/all_to_all | solution.py:93
  82.3 0.2 reshape.128
  82.7 0.3 all_to_all.22
  82.9 0.1 multiply_reduce_fusion.4
  83.1 0.1 multiply_bitcast_fusion
  83.2 3.4 %fusion = f32[8,16,1,128]{3,2,1,0:T(1,128)S(1)} fusion(bf16[8,16,128,128]{3,2,1,0:T(8,128)(2,1)} %param.34, f32[8,16]{1,0:T(8,128)S(1)} %fusion.65, bf16[8,16,128,1]{2,0,1,3:T(8,128)(2,1)S(1)} %get-tuple-element.5), kind=kOutput, calls=%fused_computation.2 | convolution fusion | flops 8388608 | bytes 4293120 | tf_op jit(solution)/shard_map/rhk,rhkv->rhv/dot_general | solution.py:51
  86.6 0.1 broadcast_multiply_fusion
  86.8 0.0 copy-start.1
  86.8 0.0 copy-start.2
  86.8 0.0 copy-start.3
  86.8 4.3 %fusion.2 = f32[8,16,1,128]{3,2,1,0:T(1,128)S(1)} fusion(bf16[8,16,128,128]{3,2,1,0:T(8,128)(2,1)} %param.34, f32[8,16,128]{2,1,0:T(8,128)S(1)} %copy.46, f32[8,16,128]{2,1,0:T(8,128)S(1)} %copy.44, f32[8,16]{1,0:T(8,128)S(1)} %fusion.65, bf16[8,16,128,1]{2,0,1,3:T(8,128)(2,1)S(1)} %get-tuple-element.4), kind=kOutput, calls=%fused_computation.4 | convolution fusion | flops 12582912 | bytes 4424192 | tf_op jit(solution)/shard_map/rhk,rhkv->rhv/dot_general | solution.py:53
  91.1 0.0 copy-start.7
  91.1 0.1 fusion.49
  91.2 0.0 copy-done.6
  91.2 4.8 %multiply_reduce_fusion.2 = (f32[8]{0:T(128)S(1)}, f32[8,2048]{1,0:T(8,128)S(1)}) fusion(bf16[2048,2048]{1,0:T(8,128)(2,1)} %param.32, f32[8,16,1,128]{3,2,1,0:T(1,128)S(1)} %fusion.2, bf16[8,4,2048]{2,0,1:T(8,128)(2,1)S(1)} %all_to_all.22, f32[128]{0:T(128)S(1)} %copy-done.6, f32[8,16]{0,1:T(8,128)S(1)} %add_rsqrt_fusion), kind=kOutput, calls=%fused_computation.79 | convolution fusion | flops 67289080 | bytes 8561184 | tf_op jit(solution)/shard_map/dot_general | solution.py:108
  96.1 0.0 copy-done.1
  96.1 0.0 copy-done.2
  96.1 0.2 multiply_reduce_fusion.1
  96.3 0.0 copy-done.3
  96.3 0.3 fusion.8
  96.6 0.1 broadcast_in_dim.5
  96.7 0.0 copy-start.4
  96.7 28.0 %all_to_all.28 = bf16[32,8,2048]{2,1,0:T(8,128)(2,1)S(1)} all-to-all(bf16[32,8,2048]{2,1,0:T(8,128)(2,1)S(1)} %bitcast.114), channel_id=1, replica_groups=mesh['ep'=32] {'ep'}, dimensions={0} | all-to-all | bytes 2097152 | tf_op jit(solution)/shard_map/all_to_all | solution.py:121
  124.7 0.0 copy-done.7
  124.7 1.5 convolution_minimum_fusion
  126.2 0.0 copy-done
  126.2 4.0 %fusion.7 = bf16[32,8,2048]{2,1,0:T(8,128)(2,1)} fusion(bf16[512,2048]{1,0:T(8,128)(2,1)S(1)} %copy-done, bf16[2048,512]{1,0:T(8,128)(2,1)} %param.39, bf16[32,8,2048]{2,1,0:T(8,128)(2,1)S(1)} %all_to_all.28, f32[256,512]{1,0:T(8,128)} %convolution_minimum_fusion), kind=kOutput, calls=%fused_computation.10 | convolution fusion | flops 1075445760 | bytes 6815744 | tf_op jit(solution)/shard_map/dot_general | solution.py:127
  130.3 0.0 copy-start.5
  130.3 3.6 %all-to-all-start.2 = ((bf16[32,8,2048]{2,1,0:T(8,128)(2,1)}), bf16[32,8,2048]{2,1,0:T(8,128)(2,1)S(1)}, u32[]{:S(2)}, u32[]{:S(2)}) async-start(bf16[32,8,2048]{2,1,0:T(8,128)(2,1)} %fusion.7), calls=%async_computation.2 | async-start | bytes 2097152 | tf_op jit(solution)/shard_map/all_to_all | solution.py:128
  133.9 0.0 copy-done.4
  133.9 0.1 copy.55
  134.0 0.1 iota_compare_fusion
  134.1 0.1 fusion.62
  134.2 6.0 %fusion.1 = bf16[8,16,128,128]{3,2,1,0:T(8,128)(2,1)} fusion(bf16[8,16,128,128]{3,2,1,0:T(8,128)(2,1)} %param.34, f32[8,16,128]{2,1,0:T(8,128)S(1)} %copy.46, f32[8,16,128]{2,1,0:T(8,128)S(1)} %copy.44, f32[8,16]{1,0:T(8,128)S(1)} %fusion.65), kind=kLoop, calls=%fused_computation.3 | loop fusion | flops 10485760 | bytes 8520192 | tf_op jit(solution)/shard_map/convert_element_type | solution.py:56
  140.2 19.9 %all-to-all-done.2 = bf16[32,8,2048]{2,1,0:T(8,128)(2,1)S(1)} async-done(((bf16[32,8,2048]{2,1,0:T(8,128)(2,1)}), bf16[32,8,2048]{2,1,0:T(8,128)(2,1)S(1)}, u32[]{:S(2)}, u32[]{:S(2)}) %all-to-all-start.2) | async-done | bytes 1048608 | tf_op jit(solution)/shard_map/all_to_all | solution.py:128
  160.1 0.2 convert_reduce_fusion
  160.3 0.5 multiply_reduce_fusion
  160.7 0.0 copy-done.5
  160.8 0.7 add_convert_fusion
  (14 shorter events, 0.2 us)
Async XLA Ops:
  7.2 119.1 %copy-start = (bf16[512,2048]{1,0:T(8,128)(2,1)S(1)}, bf16[512,2048]{1,0:T(8,128)(2,1)}, u32[]{:S(2)}) copy-start(bf16[512,2048]{1,0:T(8,128)(2,1)} %param.40) | copy-start | bytes 6291460
  7.2 60.6 %all-gather.2.cloned.1.call-start = ((), (), s32[]{:S(2)}) async-start(), calls=%async_computation.3 | async-start | bytes 1081344 | tf_op jit(solution)/shard_map/all_gather | solution.py:89
  69.5 21.7 %copy-start.6 = (f32[128]{0:T(128)S(1)}, f32[128]{0:T(128)}, u32[]{:S(2)}) copy-start(f32[128]{0:T(128)} %param.31) | copy-start | bytes 1540
  70.5 11.8 %all-to-all-start = ((bf16[32,2,1024]{2,1,0:T(2,128)(2,1)}), bf16[32,2,1024]{2,1,0:T(2,128)(2,1)S(1)}, u32[]{:S(2)}, u32[]{:S(2)}) async-start(bf16[32,2,1024]{2,1,0:T(2,128)(2,1)} %reshape.127), calls=%async_computation | async-start | bytes 262144 | tf_op jit(solution)/shard_map/all_to_all | solution.py:93
  86.8 9.3 %copy-start.1 = (bf16[8,2048]{1,0:T(8,128)(2,1)S(1)}, bf16[8,2048]{1,0:T(8,128)(2,1)}, u32[]{:S(2)}) copy-start(bf16[8,2048]{1,0:T(8,128)(2,1)} %param.21) | copy-start | bytes 98308
  86.8 9.3 %copy-start.2 = (f32[2048]{0:T(1024)S(1)}, f32[2048]{0:T(1024)}, u32[]{:S(2)}) copy-start(f32[2048]{0:T(1024)} %param.33) | copy-start | bytes 24580
  86.8 9.5 %copy-start.3 = (f32[2048]{0:T(1024)S(1)}, f32[2048]{0:T(1024)}, u32[]{:S(2)}) copy-start(f32[2048]{0:T(1024)} %param.35) | copy-start | bytes 24580
  91.1 33.6 %copy-start.7 = (bf16[2048,512]{1,0:T(8,128)(2,1)S(1)}, bf16[2048,512]{1,0:T(8,128)(2,1)}, u32[]{:S(2)}) copy-start(bf16[2048,512]{1,0:T(8,128)(2,1)} %param.38) | copy-start | bytes 6291460
  96.7 37.2 %copy-start.4 = (f32[8,4]{0,1:T(4,128)S(1)}, f32[8,4]{0,1:T(4,128)}, u32[]{:S(2)}) copy-start(f32[8,4]{0,1:T(4,128)} %param.37) | copy-start | bytes 388
  130.3 30.5 %copy-start.5 = (f32[2048]{0:T(1024)S(1)}, f32[2048]{0:T(1024)}, u32[]{:S(2)}) copy-start(f32[2048]{0:T(1024)} %param.41) | copy-start | bytes 24580
  130.3 29.8 %all-to-all-start.2 = ((bf16[32,8,2048]{2,1,0:T(8,128)(2,1)}), bf16[32,8,2048]{2,1,0:T(8,128)(2,1)S(1)}, u32[]{:S(2)}, u32[]{:S(2)}) async-start(bf16[32,8,2048]{2,1,0:T(8,128)(2,1)} %fusion.7), calls=%async_computation.2 | async-start | bytes 2097152 | tf_op jit(solution)/shard_map/all_to_all | solution.py:128
Sparse Core Ops, SparseCore 0:
  11.4 56.3 all-gather.1
where the time goes:
time: 169 us; the launch traced here: 168 us
  waiting for transfers between devices  80.7 us (48%)
  blocking collectives  28 us (17%)
  matrix products  22.7 us (13%)
  between operations  14.3 us (8%)
  other arithmetic  12.5 us (7%)
  starting transfers between devices  7.24 us (4%)
  local copies, waits for them, and re-layouts  2.96 us (2%)
    all_gather x1, waiting for transfers between devices, shards(): lax.all_gather(normed, 'ep', axis=0, tiled=True)  54.4 us
    all_to_all x1, blocking collectives, shards(): block = lax.all_to_all(sent, 'ep', split_axis=0, concat_axis=0, tiled=True)  28 us
    all_to_all x1, waiting for transfers between devices, shards(): lax.all_to_all(partial_value.reshape(block.shape), 'ep', split_axis=0, co...  19.9 us
    all_to_all x1, waiting for transfers between devices, shards(): lax.all_to_all(columns, 'ep', split_axis=0, concat_axis=2, tiled=True)  6.41 us
    convert_element_type x1, other arithmetic, delta_step(): return (gated.astype(jnp.bfloat16), held.astype(jnp.bfloat16))  5.95 us
    dot_general x1, matrix products, shards(): branch = jnp.dot(mixed, w_out, preferred_element_type=jnp.float32)  4.85 us
    dot_general x1, matrix products, delta_step(): output = jnp.einsum('rhk,rhkv->rhv', query, held)  4.26 us
    dot_general x1, matrix products, shards(): jnp.dot(hidden, w_down, preferred_element_type=jnp.float32)  4.05 us
  transfers between devices with their start and end apart: 3, of which 3 were waited for; matrix products, arithmetic and copies ran while one was open for 7% of the time, Pallas kernels for 0%

commit v1 on v0

v1 whole, which is shorter than its diff:
```python
import functools

import jax
import jax.numpy as jnp
from jax import lax
from jax.experimental import pallas as pl
from jax.experimental.pallas import tpu as pltpu
from jax.sharding import PartitionSpec as P

H = 16
HD = 128
PIECES = 4
TOPK = 4
LANES = 128
TAIL = 2 * LANES
MESH = pl.DeviceIdType.MESH

EPS = 1e-06
LIMIT = 7.0
ALPHA = 1.702


def rms_scale(values):
    return values * lax.rsqrt(jnp.mean(values * values, axis=-1, keepdims=True) + EPS)


def clamped_unit(gate, upper):
    glu = jnp.minimum(gate, LIMIT)
    linear = jnp.clip(upper, -LIMIT, LIMIT)
    return glu * jax.nn.sigmoid(ALPHA * glu) * (linear + 1.0)


def delta_step(
    q_raw, k_raw, v_raw, z_raw, decay_in, beta_in, state, decay_scale, decay_bias, head_gain
):
    count = q_raw.shape[0]
    query = jax.nn.silu(q_raw.astype(jnp.float32)).reshape(count, H, HD)
    query = query * lax.rsqrt(jnp.sum(query * query, axis=-1, keepdims=True) + EPS) * HD ** (-0.5)
    keys = jax.nn.silu(k_raw.astype(jnp.float32)).reshape(count, H, HD)
    keys = keys * lax.rsqrt(jnp.sum(keys * keys, axis=-1, keepdims=True) + EPS)
    values = jax.nn.silu(v_raw.astype(jnp.float32)).reshape(count, H, HD)
    decay = -decay_scale * jax.nn.softplus(decay_in + decay_bias)
    beta = jax.nn.sigmoid(beta_in)
    held = state.astype(jnp.float32) * jnp.exp(decay)[:, :, None, None]
    guess = jnp.einsum("rhk,rhkv->rhv", keys, held)
    held = held + jnp.einsum("rhk,rhv->rhkv", keys, beta[:, :, None] * (values - guess))
    output = jnp.einsum("rhk,rhkv->rhv", query, held)
    output = rms_scale(output) * head_gain
    gated = output.reshape(count, H * HD) * jax.nn.silu(z_raw.astype(jnp.float32))
    return (gated.astype(jnp.bfloat16), held.astype(jnp.bfloat16))

def flipped(value, distance):
    bit = 1
    while bit <= distance:
        if distance & bit:
            value = value + bit - 2 * bit * (lax.rem(value // bit, 2))
        bit *= 2
    return value


class Place:
    def __init__(self, devices):
        self.devices = devices
        self.layers = devices // 8
        self.me = lax.axis_index("ep")
        self.core = lax.rem(self.me, 2)
        self.x = lax.rem(self.me // 2, 2)
        self.y = lax.rem(self.me // 4, 2)
        self.z = self.me // 8

    def at(self, distance=0, y=0, x=0, core=0):
        z = flipped(self.z, distance)
        return (
            z * 8
            + flipped(self.y, y) * 4
            + flipped(self.x, x) * 2
            + flipped(self.core, core)
        )

    def partners(self):
        return [self.at(d) for d in range(1, self.layers)] + [
            self.at(y=1),
            self.at(x=1),
            self.at(core=1),
        ]


def greet(place):
    barrier = pltpu.get_barrier_semaphore()
    for partner in place.partners():
        pl.semaphore_signal(barrier, inc=1, device_id=(partner,), device_id_type=MESH)
    return lambda: pl.semaphore_wait(barrier, len(place.partners()))


def remote(source, target, send_sem, recv_sem, device):
    return pltpu.make_async_remote_copy(
        src_ref=source,
        dst_ref=target,
        send_sem=send_sem,
        recv_sem=recv_sem,
        device_id=(device,),
        device_id_type=MESH,
    )


def gather_sends(devices):
    layers = devices // 8
    return layers - 1 + 3 * layers + devices // 2


def gather_blocks(place, buf, send_sems, recv_sems):
    started = []

    def push(block, device):
        copy = remote(
            buf.at[block], buf.at[block], send_sems.at[len(started)], recv_sems.at[block], device
        )
        copy.start()
        started.append(copy)

    def arrive(block):
        remote(
            buf.at[block], buf.at[block], send_sems.at[0], recv_sems.at[block], place.at(core=1)
        ).wait_recv()

    def spread(distance):
        block = place.at(distance)
        push(block, place.at(x=1))
        push(block, place.at(y=1))
        push(block, place.at(core=1))

    def onward(distance):
        across_x, across_y = place.at(distance, x=1), place.at(distance, y=1)
        arrive(across_x)
        if distance % 2 == 0:
            push(across_x, place.at(y=1))
        push(across_x, place.at(core=1))
        arrive(across_y)
        if distance % 2 == 1:
            push(across_y, place.at(x=1))
        push(across_y, place.at(core=1))

    layers = place.layers
    for distance in range(layers - 1, 0, -1):
        push(place.me, place.at(distance))
    spread(0)
    for distance in range(1, layers):
        arrive(place.at(distance))
        spread(distance)
        onward(distance - 1)
    onward(layers - 1)
    for distance in range(layers):
        diagonal = place.at(distance, y=1, x=1)
        arrive(diagonal)
        push(diagonal, place.at(core=1))
    for distance in range(layers):
        for y in range(2):
            for x in range(2):
                arrive(place.at(distance, y, x, 1))
    return started


def settle(started):
    for copy in started:
        copy.wait_send()


def reduce_blocks(place, mine, paired, total, second, third, fourth, sems):
    pair_recv, send_sems, second_recv, third_recv, fourth_recv = sems
    started = []
    layers = place.layers

    def push(source, target, recv_sem, device):
        copy = remote(source, target, send_sems.at[len(started)], recv_sem, device)
        copy.start()
        started.append(copy)

    def arrive(target, recv_sem):
        remote(target, target, send_sems.at[0], recv_sem, place.at(core=1)).wait_recv()

    def wide(block):
        return block.astype(jnp.float32)

    order = list(range(layers - 1, -1, -1))
    for distance in order:
        for y, x in ((1, 1), (0, 1), (1, 0), (0, 0)):
            k = place.at(distance, y, x) // 2
            arrive(paired.at[k], pair_recv.at[k])
            total[k] = (wide(mine[k]) + wide(paired[k])).astype(jnp.bfloat16)
    for distance in order:
        if distance % 2 == 0:
            first, far, near = place.at(y=1), (1, 1), (1, 0)
        else:
            first, far, near = place.at(x=1), (1, 1), (0, 1)
        for slot, (y, x) in ((1, far), (0, near)):
            k = place.at(distance, y, x) // 2
            at = 2 * distance + slot
            push(total.at[k], second.at[at], second_recv.at[at], first)
    for distance in order:
        if distance % 2 == 0:
            then, (y, x) = place.at(x=1), (0, 1)
        else:
            then, (y, x) = place.at(y=1), (1, 0)
        k = place.at(distance, y, x) // 2
        at = 2 * distance + 1
        arrive(second.at[at], second_recv.at[at])
        total[k] = (wide(total[k]) + wide(second[at])).astype(jnp.bfloat16)
        push(total.at[k], third.at[distance], third_recv.at[distance], then)
    for distance in order:
        k = place.at(distance) // 2
        at = 2 * distance
        arrive(second.at[at], second_recv.at[at])
        arrive(third.at[distance], third_recv.at[distance])
        value = wide(total[k]) + wide(second[at]) + wide(third[distance])
        if distance > 0:
            total[k] = value.astype(jnp.bfloat16)
            push(total.at[k], fourth.at[distance], fourth_recv.at[distance], place.at(distance))
    for distance in range(1, layers):
        arrive(fourth.at[distance], fourth_recv.at[distance])
        value = value + wide(fourth[distance])
    return value, started


def dot_t(left, right):
    return lax.dot_general(
        left, right, (((1,), (1,)), ((), ())), preferred_element_type=jnp.float32
    )


def project_kernel(
    devices,
    x_ref,
    gain_ref,
    routes_ref,
    logits_ref,
    q_ref,
    k_ref,
    v_ref,
    z_ref,
    decay_ref,
    beta_ref,
    columns_ref,
    shares_ref,
    decay_out,
    beta_out,
    buf,
    weights,
    send_sems,
    recv_sems,
    load_sems,
):
    place = Place(devices)
    ready = greet(place)
    width = x_ref.shape[1]
    own = q_ref.shape[0]
    loads = [
        pltpu.make_async_copy(ref, weights.at[pl.ds(i * own, own)], load_sems.at[i])
        for i, ref in enumerate((q_ref, k_ref, v_ref, z_ref))
    ]
    for load in loads:
        load.start()
    normed = (rms_scale(x_ref[...].astype(jnp.float32)) * gain_ref[...]).astype(jnp.bfloat16)
    raised = jnp.exp(logits_ref[...])
    shares = raised / jnp.sum(raised, axis=-1, keepdims=True)
    routes = routes_ref[...]
    lane = lax.broadcasted_iota(jnp.int32, (x_ref.shape[0], LANES), 1)
    share = jnp.zeros(lane.shape, jnp.float32)
    for j in range(routes.shape[1]):
        share = share + jnp.where(lane == routes[:, j : j + 1], shares[:, j : j + 1], 0.0)
    high = share.astype(jnp.bfloat16)
    low = (share - high.astype(jnp.float32)).astype(jnp.bfloat16)
    buf[place.me, :, 0:width] = normed
    buf[place.me, :, width : width + LANES] = high
    buf[place.me, :, width + LANES : width + TAIL] = low
    decay_out[...] = dot_t(normed, decay_ref[...])
    beta_out[...] = dot_t(normed, beta_ref[...])
    ready()
    started = gather_blocks(place, buf, send_sems, recv_sems)
    for load in loads:
        load.wait()
    count = x_ref.shape[0]
    rows = buf[:, :, 0:width].reshape(devices * count, width)
    columns = dot_t(rows, weights[...])
    columns_ref[...] = columns.astype(jnp.bfloat16).reshape(columns_ref.shape)
    shares_ref[...] = buf[:, :, width:]
    settle(started)


def project(devices, x, gain, routes, logits, w_query, w_key, w_value, w_outgate, w_decay, w_beta):
    count, width = x.shape
    own = w_query.shape[1]
    vmem = pl.BlockSpec(memory_space=pltpu.VMEM)
    hbm = pl.BlockSpec(memory_space=pl.ANY)
    heads = w_decay.shape[1]
    return pl.pallas_call(
        functools.partial(project_kernel, devices),
        out_shape=(
            jax.ShapeDtypeStruct((devices, count, 4 * own), jnp.bfloat16),
            jax.ShapeDtypeStruct((devices, count, TAIL), jnp.bfloat16),
            jax.ShapeDtypeStruct((count, heads), jnp.float32),
            jax.ShapeDtypeStruct((count, heads), jnp.float32),
        ),
        in_specs=[vmem] * 4 + [hbm] * 4 + [vmem] * 2,
        out_specs=(vmem,) * 4,
        scratch_shapes=[
            pltpu.VMEM((devices, count, width + TAIL), jnp.bfloat16),
            pltpu.VMEM((4 * own, width), jnp.bfloat16),
            pltpu.SemaphoreType.DMA((gather_sends(devices),)),
            pltpu.SemaphoreType.DMA((devices,)),
            pltpu.SemaphoreType.DMA((4,)),
        ],
        compiler_params=pltpu.CompilerParams(
            collective_id=0, has_side_effects=True, vmem_limit_bytes=32 << 20
        ),
    )(
        x,
        gain[None],
        routes,
        logits,
        w_query.T,
        w_key.T,
        w_value.T,
        w_outgate.T,
        w_decay.T,
        w_beta.T,
    )


def expert_kernel(
    devices,
    branch_ref,
    x_ref,
    gain_mix_ref,
    gain_pre_ref,
    gain_post_ref,
    shares_ref,
    gate_hbm,
    up_hbm,
    down_hbm,
    result_ref,
    buf,
    gate,
    up,
    down,
    hidden,
    weight,
    theirs,
    mine,
    paired,
    total,
    second,
    third,
    fourth,
    gather_send,
    gather_recv,
    load_sems,
    pair_send,
    pair_recv,
    sum_send,
    second_recv,
    third_recv,
    fourth_recv,
):
    place = Place(devices)
    ready = greet(place)
    loads = [
        pltpu.make_async_copy(source, target, load_sems.at[i])
        for i, (source, target) in enumerate(((gate_hbm, gate), (up_hbm, up), (down_hbm, down)))
    ]
    for load in loads:
        load.start()
    count, width = x_ref.shape
    pieces = gate.shape[1]
    pairs = devices // 2
    x_second = x_ref[...].astype(jnp.float32) + rms_scale(branch_ref[...]) * gain_mix_ref[...]
    buf[place.me] = (rms_scale(x_second) * gain_pre_ref[...]).astype(jnp.bfloat16)
    ready()
    started = gather_blocks(place, buf, gather_send, gather_recv)
    share = shares_ref[:, :, 0:LANES].astype(jnp.float32) + shares_ref[:, :, LANES:].astype(
        jnp.float32
    )
    share = share.reshape(devices * count, LANES)
    lane = lax.broadcasted_iota(jnp.int32, share.shape, 1)
    share = jnp.sum(jnp.where(lane == place.me // PIECES, share, 0.0), axis=1, keepdims=True)
    weight[...] = jnp.broadcast_to(share, (devices * count, LANES)).reshape(weight.shape)
    loads[0].wait()
    loads[1].wait()
    rows = buf[...].reshape(devices * count, width)
    step = 256
    for j in range(0, pieces, step):
        gated = clamped_unit(
            jnp.dot(rows, gate[:, j : j + step], preferred_element_type=jnp.float32),
            jnp.dot(rows, up[:, j : j + step], preferred_element_type=jnp.float32),
        )
        hidden[:, :, :, j : j + step] = gated.astype(jnp.bfloat16).reshape(
            pairs, 2, count, step
        )
    loads[2].wait()

    def parts(core, out):
        units = hidden[:, core].reshape(pairs * count, pieces)
        scale = weight[:, core].reshape(pairs * count, LANES)[:, 0:1]
        for j in range(0, width, 512):
            part = jnp.dot(units, down[:, j : j + 512], preferred_element_type=jnp.float32)
            out[:, :, j : j + 512] = (
                (part * scale).astype(jnp.bfloat16).reshape(pairs, count, 512)
            )

    parts(1 - place.core, theirs)
    sent = []
    for distance in range(place.layers - 1, -1, -1):
        for y, x in ((1, 1), (0, 1), (1, 0), (0, 0)):
            k = place.at(distance, y, x) // 2
            copy = remote(
                theirs.at[k],
                paired.at[k],
                pair_send.at[len(sent)],
                pair_recv.at[k],
                place.at(core=1),
            )
            copy.start()
            sent.append(copy)
    parts(place.core, mine)
    moe, more = reduce_blocks(
        place,
        mine,
        paired,
        total,
        second,
        third,
        fourth,
        (pair_recv, sum_send, second_recv, third_recv, fourth_recv),
    )
    result_ref[...] = (x_second + rms_scale(moe) * gain_post_ref[...]).astype(jnp.bfloat16)
    settle(started + sent + more)


def experts_part(
    devices, branch, x, gain_mix, gain_pre, gain_post, shares, w_gate, w_up, w_down
):
    count, width = x.shape
    layers = devices // 8
    pairs = devices // 2
    pieces = w_gate.shape[1]
    vmem = pl.BlockSpec(memory_space=pltpu.VMEM)
    hbm = pl.BlockSpec(memory_space=pl.ANY)
    dma = pltpu.SemaphoreType.DMA

    def blocks(number):
        return pltpu.VMEM((number, count, width), jnp.bfloat16)

    return pl.pallas_call(
        functools.partial(expert_kernel, devices),
        out_shape=jax.ShapeDtypeStruct((count, width), jnp.bfloat16),
        in_specs=[vmem] * 6 + [hbm] * 3,
        out_specs=vmem,
        scratch_shapes=[
            blocks(devices),
            pltpu.VMEM(w_gate.shape, jnp.bfloat16),
            pltpu.VMEM(w_up.shape, jnp.bfloat16),
            pltpu.VMEM(w_down.shape, jnp.bfloat16),
            pltpu.VMEM((pairs, 2, count, pieces), jnp.bfloat16),
            pltpu.VMEM((pairs, 2, count, LANES), jnp.float32),
            blocks(pairs),
            blocks(pairs),
            blocks(pairs),
            blocks(pairs),
            blocks(2 * layers),
            blocks(layers),
            blocks(layers),
            dma((gather_sends(devices),)),
            dma((devices,)),
            dma((3,)),
            dma((pairs,)),
            dma((pairs,)),
            dma((4 * layers,)),
            dma((2 * layers,)),
            dma((layers,)),
            dma((layers,)),
        ],
        compiler_params=pltpu.CompilerParams(
            collective_id=1, has_side_effects=True, vmem_limit_bytes=48 << 20
        ),
    )(
        branch,
        x,
        gain_mix[None],
        gain_pre[None],
        gain_post[None],
        shares,
        w_gate,
        w_up,
        w_down,
    )


def shards(
    residual_in,
    gain_mix_pre,
    w_query,
    w_key,
    w_value,
    w_outgate,
    w_decay,
    w_beta,
    decay_scale,
    decay_bias,
    head_gain,
    w_out,
    gain_mix_post,
    state_cache,
    gain_ffn_pre,
    routes,
    route_logits,
    w_gate,
    w_up,
    w_down,
    gain_ffn_post,
):
    devices = lax.axis_size("ep")
    columns, shares, decay_in, beta_in = project(
        devices,
        residual_in,
        gain_mix_pre,
        routes,
        route_logits,
        w_query,
        w_key,
        w_value,
        w_outgate,
        w_decay,
        w_beta,
    )
    count = residual_in.shape[0]
    joined = lax.all_to_all(columns, "ep", split_axis=0, concat_axis=0, tiled=True)
    joined = joined.reshape(devices, count, 4, -1).transpose(2, 1, 0, 3).reshape(4, count, H * HD)
    mixed, new_state = delta_step(
        joined[0],
        joined[1],
        joined[2],
        joined[3],
        decay_in,
        beta_in,
        state_cache,
        decay_scale,
        decay_bias,
        head_gain,
    )
    branch = jnp.dot(mixed, w_out, preferred_element_type=jnp.float32)
    result = experts_part(
        devices,
        branch,
        residual_in,
        gain_mix_post,
        gain_ffn_pre,
        gain_ffn_post,
        shares,
        w_gate,
        w_up,
        w_down,
    )
    return (result, new_state)


def solution(mesh):
    in_specs = (
        P("ep", None),
        P(),
        P(None, "ep"),
        P(None, "ep"),
        P(None, "ep"),
        P(None, "ep"),
        P(),
        P(),
        P(),
        P(),
        P(),
        P(),
        P(),
        P("ep", None, None, None),
        P(),
        P("ep", None),
        P("ep", None),
        P(None, "ep"),
        P(None, "ep"),
        P("ep", None),
        P(),
    )
    out_specs = (P("ep", None), P("ep", None, None, None))
    return jax.shard_map(shards, mesh=mesh, in_specs=in_specs, out_specs=out_specs, check_vma=False)
```

time: 169 us -> 93.6 us (0.55)
  waiting for transfers between devices: 80.7 us -> 6.87 us
  Pallas kernels: 0 us -> 50.6 us
  blocking collectives: 28 us -> 0 us
  between operations: 14.3 us -> 0.82 us
  matrix products: 22.7 us -> 12.1 us
  local copies, waits for them, and re-layouts: 2.96 us -> 10.1 us
  other arithmetic: 12.5 us -> 8.02 us
  starting transfers between devices: 7.24 us -> 4.37 us
    all_gather x1 -> x0, waiting for transfers between devices: 54.4 us -> none  [shards(): lax.all_gather(normed, 'ep', axis=0, tiled=True)]
    pallas_call x0 -> x2, Pallas kernels: none -> 50.6 us  [the longest x1 30.7 us: experts_part(): pl.pallas_call(functools.partial(expert_kernel, devices), out_shape=jax.S...]
    all_to_all x1 -> x0, blocking collectives: 28 us -> none  [shards(): block = lax.all_to_all(sent, 'ep', split_axis=0, concat_axis=0, tiled=True)]
    all_to_all x2 -> x1, waiting for transfers between devices: 26.3 us -> 6.87 us  [shards(): lax.all_to_all(columns, 'ep', split_axis=0, concat_axis=0, tiled=True)]
    dot_general x7 -> x0, matrix products: 8.41 us -> none  [the longest x1 4.05 us: shards(): jnp.dot(hidden, w_down, preferred_element_type=jnp.float32)]
    unnamed x19 -> x35, local copies, waits for them, and re-layouts: 1.88 us -> 9.1 us
    all_to_all x2 -> x1, starting transfers between devices: 7.2 us -> 4.37 us  [shards(): lax.all_to_all(columns, 'ep', split_axis=0, concat_axis=0, tiled=True)]
    convert_element_type x4 -> x1, other arithmetic: 2.25 us -> 0.05 us  [delta_step(): values = jax.nn.silu(v_raw.astype(jnp.float32)).reshape(count, H, HD)]
  transfers between devices with their start and end apart: 3 -> 1, of which waited for: 3 -> 1; matrix products, arithmetic and copies ran while one was open for 7% -> 1% of each run, Pallas kernels for 0% -> 0%
where the time goes in v1:
time: 93.6 us; the launch traced here: 92.9 us
  Pallas kernels  50.6 us (54%)
  matrix products  12.1 us (13%)
  local copies, waits for them, and re-layouts  10.1 us (11%)
  other arithmetic  8.02 us (9%)
  waiting for transfers between devices  6.87 us (7%)
  starting transfers between devices  4.37 us (5%)
    pallas_call x1, Pallas kernels, experts_part(): pl.pallas_call(functools.partial(expert_kernel, devices), out_shape=jax.S...  30.7 us
    pallas_call x1, Pallas kernels, project(): pl.pallas_call(functools.partial(project_kernel, devices), out_shape=(jax...  19.9 us
    unnamed x35, local copies, waits for them, and re-layouts  9.1 us
    all_to_all x1, waiting for transfers between devices, shards(): lax.all_to_all(columns, 'ep', split_axis=0, concat_axis=0, tiled=True)  6.87 us
    convert_element_type x1, other arithmetic, delta_step(): return (gated.astype(jnp.bfloat16), held.astype(jnp.bfloat16))  6.04 us
    dot_general x1, matrix products, shards(): branch = jnp.dot(mixed, w_out, preferred_element_type=jnp.float32)  4.76 us
    all_to_all x1, starting transfers between devices, shards(): lax.all_to_all(columns, 'ep', split_axis=0, concat_axis=0, tiled=True)  4.37 us
    dot_general x1, matrix products, delta_step(): output = jnp.einsum('rhk,rhkv->rhv', query, held)  3.78 us
  transfers between devices with their start and end apart: 1, of which 1 were waited for; matrix products, arithmetic and copies ran while one was open for 1% of the time, Pallas kernels for 0%

profile of v1, /device:TPU:0, one launch (start us, length us, event | category | flops | bytes accessed | tf_op | source)
XLA Modules:
  0.0 92.9 jit_solution(4645056547340228030)
XLA Ops:
  0.6 0.8 copy.36.routes_ref
  1.4 0.8 copy.37.logits_ref
  2.1 0.0 copy-start.2
  2.1 0.9 %copy-done.2 = bf16[2048,64]{0,1:T(8,128)(2,1)S(1)} copy-done((bf16[2048,64]{0,1:T(8,128)(2,1)S(1)}, bf16[2048,64]{0,1:T(8,128)(2,1)}, u32[]{:S(2)}) %copy-start.2) | copy-done | bytes 262168
  3.1 0.0 copy-start.3
  3.1 0.9 %copy-done.3 = bf16[2048,64]{0,1:T(8,128)(2,1)S(1)} copy-done((bf16[2048,64]{0,1:T(8,128)(2,1)S(1)}, bf16[2048,64]{0,1:T(8,128)(2,1)}, u32[]{:S(2)}) %copy-start.3) | copy-done | bytes 262168
  4.0 0.0 copy-start.4
  4.0 0.9 %copy-done.4 = bf16[2048,64]{0,1:T(8,128)(2,1)S(1)} copy-done((bf16[2048,64]{0,1:T(8,128)(2,1)S(1)}, bf16[2048,64]{0,1:T(8,128)(2,1)}, u32[]{:S(2)}) %copy-start.4) | copy-done | bytes 262168
  5.0 0.0 copy-start.5
  5.0 0.9 %copy-done.5 = bf16[2048,64]{0,1:T(8,128)(2,1)S(1)} copy-done((bf16[2048,64]{0,1:T(8,128)(2,1)S(1)}, bf16[2048,64]{0,1:T(8,128)(2,1)}, u32[]{:S(2)}) %copy-start.5) | copy-done | bytes 262168
  5.9 0.0 copy-start.6
  5.9 0.8 copy-done.6
  6.7 0.0 copy-start.8
  6.7 0.8 copy-done.8
  7.5 0.0 copy-start.9
  7.5 0.8 copy-done.9
  8.4 0.0 copy-start.10
  8.4 0.7 copy-done.10
  9.1 19.9 %shard_map.212 = (bf16[32,8,256]{2,1,0:T(8,128)(2,1)}, bf16[32,8,256]{2,1,0:T(8,128)(2,1)S(1)}, f32[8,16]{1,0:T(8,128)S(1)}, f32[8,16]{1,0:T(8,128)S(1)}) custom-call(bf16[8,2048]{1,0:T(8,128)(2,1)S(1)} %copy-done.6, f32[1,2048]{1,0:T(1,128)S(1)} %bitcast.55, s32[8,4]{1,0:T(8,128)S(1)} %copy.36.routes_ref, f32[8,4]{1,0:T(8,128)S(1)} %copy.37.logits_ref, ...), custom_call_target="tpu_custom_call" | custom-call | tf_op jit(solution)/shard_map/pallas_call | solution.py:295
  29.0 4.4 %all-to-all-start = ((bf16[32,8,256]{2,1,0:T(8,128)(2,1)}), bf16[32,8,256]{2,1,0:T(8,128)(2,1)S(1)}, u32[]{:S(2)}, u32[]{:S(2)}) async-start(bf16[32,8,256]{2,1,0:T(8,128)(2,1)} %get-tuple-element.6), calls=%async_computation | async-start | bytes 262144 | tf_op jit(solution)/shard_map/all_to_all | solution.py:535
  33.4 0.7 neg.34
  34.1 0.7 fusion.16
  34.7 6.9 %all-to-all-done = bf16[32,8,256]{2,1,0:T(8,128)(2,1)S(1)} async-done(((bf16[32,8,256]{2,1,0:T(8,128)(2,1)}), bf16[32,8,256]{2,1,0:T(8,128)(2,1)S(1)}, u32[]{:S(2)}, u32[]{:S(2)}) %all-to-all-start) | async-done | bytes 131104 | tf_op jit(solution)/shard_map/all_to_all | solution.py:535
  41.6 0.2 reshape.60
  41.8 0.1 copy.53
  41.9 0.2 multiply_reduce_fusion
  42.0 0.1 slice_convert_fusion.1
  42.1 0.1 copy.41
  42.2 0.1 copy.42
  42.3 0.1 copy.39
  42.4 0.1 copy.40
  42.5 0.1 reshape.64
  42.6 0.1 reshape.65
  42.7 0.1 reshape.63
  42.7 0.1 reshape.62
  42.8 0.0 copy-start.14
  42.8 0.1 multiply_multiply_fusion
  42.9 3.6 %fusion = f32[8,16,1,128]{3,2,1,0:T(1,128)S(1)} fusion(f32[8,16,128,1]{2,3,1,0:T(1,128)S(1)} %bitcast.61, bf16[8,16,128,128]{3,2,1,0:T(8,128)(2,1)} %param.34, f32[8,16]{1,0:T(8,128)S(1)} %get-tuple-element.16), kind=kOutput, calls=%fused_computation.2 | convolution fusion | flops 8388608 | bytes 4325888 | tf_op jit(solution)/shard_map/rhk,rhkv->rhv/dot_general | solution.py:45
  46.5 0.1 subtract_multiply_fusion
  46.6 0.0 copy-start.15
  46.6 6.0 %fusion.1 = bf16[8,16,128,128]{3,2,1,0:T(8,128)(2,1)} fusion(bf16[8,16,128,128]{3,2,1,0:T(8,128)(2,1)} %param.34, f32[8,16,128]{2,1,0:T(8,128)S(1)} %subtract_multiply_fusion, f32[8,16,128]{2,1,0:T(8,128)S(1)} %multiply_multiply_fusion, f32[8,16]{1,0:T(8,128)S(1)} %get-tuple-element.16), kind=kLoop, calls=%fused_computation.3 | loop fusion | flops 10485760 | bytes 8520192 | tf_op jit(solution)/shard_map/convert_element_type | solution.py:50
  52.7 0.1 multiply_multiply_fusion.1
  52.8 0.0 copy-done.14
  52.8 3.8 %fusion.2 = f32[8,16,1,128]{3,2,1,0:T(1,128)S(1)} fusion(f32[8,16,128,1]{2,3,1,0:T(1,128)S(1)} %bitcast.65, bf16[8,16,128,128]{3,2,1,0:T(8,128)(2,1)S(1)} %copy-done.14, f32[8,16,128]{2,1,0:T(8,128)S(1)} %subtract_multiply_fusion, f32[8,16,128]{2,1,0:T(8,128)S(1)} %multiply_multiply_fusion, f32[8,16]{1,0:T(8,128)S(1)} %get-tuple-element.16), kind=kOutput, calls=%fused_computation.4 | convolution fusion | flops 12582912 | bytes 4456960 | tf_op jit(solution)/shard_map/rhk,rhkv->rhv/dot_general | solution.py:47
  56.6 0.0 copy-start
  56.6 0.0 copy-start.7
  56.6 0.0 copy-start.11
  56.6 0.0 copy-start.12
  56.6 0.0 copy-start.13
  56.6 0.1 fusion.8
  56.7 0.1 copy.43
  56.8 0.1 copy.44
  56.9 0.0 copy-done.15
  56.9 0.0 copy-start.1
  56.9 4.8 %fusion.10.branch_ref = f32[8,2048]{1,0:T(8,128)S(1)} fusion(bf16[2048,2048]{1,0:T(8,128)(2,1)} %param.32, f32[8,2048]{1,0:T(8,128)S(1)} %reshape.65, f32[8,16,1,128]{3,2,1,0:T(1,128)S(1)} %fusion.2, f32[128]{0:T(128)S(1)} %copy-done.15, f32[8,16]{0,1:T(8,128)S(1)} %copy.44), kind=kOutput, calls=%fused_computation.25 | convolution fusion | flops 67239936 | bytes 8586240 | tf_op jit(solution)/shard_map/dot_general | solution.py:549
  61.6 0.0 copy-done
  61.6 0.0 copy-done.7
  61.6 0.0 copy-done.11
  61.6 0.0 copy-done.12
  61.6 0.0 copy-done.13
  61.7 0.0 copy-done.1
  61.7 30.7 %shard_map.213 = bf16[8,2048]{1,0:T(8,128)(2,1)S(1)} custom-call(f32[8,2048]{1,0:T(8,128)S(1)} %fusion.10.branch_ref, bf16[8,2048]{1,0:T(8,128)(2,1)S(1)} %copy-done.7, f32[1,2048]{1,0:T(1,128)S(1)} %bitcast.56, f32[1,2048]{1,0:T(1,128)S(1)} %bitcast.57, f32[1,2048]{1,0:T(1,128)S(1)} %bitcast.58, bf16[32,8,256]{2,1,0:T(8,128)(2,1)S(1)} %get-tuple-element.9.shares_ref, ...), custom_call_target="tpu_custom_call" | custom-call | tf_op jit(solution)/shard_map/pallas_call | solution.py:452
  92.3 0.6 copy.55
  (5 shorter events, 0.1 us)
Async XLA Ops:
  2.1 0.9 %copy-start.2 = (bf16[2048,64]{0,1:T(8,128)(2,1)S(1)}, bf16[2048,64]{0,1:T(8,128)(2,1)}, u32[]{:S(2)}) copy-start(bf16[2048,64]{0,1:T(8,128)(2,1)} %param.23) | copy-start | bytes 786436
  3.1 0.9 %copy-start.3 = (bf16[2048,64]{0,1:T(8,128)(2,1)S(1)}, bf16[2048,64]{0,1:T(8,128)(2,1)}, u32[]{:S(2)}) copy-start(bf16[2048,64]{0,1:T(8,128)(2,1)} %param.24) | copy-start | bytes 786436
  4.0 0.9 %copy-start.4 = (bf16[2048,64]{0,1:T(8,128)(2,1)S(1)}, bf16[2048,64]{0,1:T(8,128)(2,1)}, u32[]{:S(2)}) copy-start(bf16[2048,64]{0,1:T(8,128)(2,1)} %param.25) | copy-start | bytes 786436
  5.0 0.9 %copy-start.5 = (bf16[2048,64]{0,1:T(8,128)(2,1)S(1)}, bf16[2048,64]{0,1:T(8,128)(2,1)}, u32[]{:S(2)}) copy-start(bf16[2048,64]{0,1:T(8,128)(2,1)} %param.26) | copy-start | bytes 786436
  5.9 0.8 copy-start.6
  6.7 0.8 copy-start.8
  7.5 0.8 copy-start.9
  8.4 0.7 copy-start.10
  29.0 12.6 %all-to-all-start = ((bf16[32,8,256]{2,1,0:T(8,128)(2,1)}), bf16[32,8,256]{2,1,0:T(8,128)(2,1)S(1)}, u32[]{:S(2)}, u32[]{:S(2)}) async-start(bf16[32,8,256]{2,1,0:T(8,128)(2,1)} %get-tuple-element.6), calls=%async_computation | async-start | bytes 262144 | tf_op jit(solution)/shard_map/all_to_all | solution.py:535
  42.8 9.9 %copy-start.14 = (bf16[8,16,128,128]{3,2,1,0:T(8,128)(2,1)S(1)}, bf16[8,16,128,128]{3,2,1,0:T(8,128)(2,1)}, u32[]{:S(2)}) copy-start(bf16[8,16,128,128]{3,2,1,0:T(8,128)(2,1)} %param.34) | copy-start | bytes 12582916
  46.6 10.2 %copy-start.15 = (f32[128]{0:T(128)S(1)}, f32[128]{0:T(128)}, u32[]{:S(2)}) copy-start(f32[128]{0:T(128)} %param.31) | copy-start | bytes 1540
  56.6 5.1 %copy-start = (bf16[2048,512]{1,0:T(8,128)(2,1)S(1)}, bf16[2048,512]{1,0:T(8,128)(2,1)}, u32[]{:S(2)}) copy-start(bf16[2048,512]{1,0:T(8,128)(2,1)} %gate_hbm.1) | copy-start | bytes 6291460
  56.6 5.1 %copy-start.7 = (bf16[8,2048]{1,0:T(8,128)(2,1)S(1)}, bf16[8,2048]{1,0:T(8,128)(2,1)}, u32[]{:S(2)}) copy-start(bf16[8,2048]{1,0:T(8,128)(2,1)} %x_ref.3) | copy-start | bytes 98308
  56.6 5.1 %copy-start.11 = (f32[2048]{0:T(1024)S(1)}, f32[2048]{0:T(1024)}, u32[]{:S(2)}) copy-start(f32[2048]{0:T(1024)} %param.33) | copy-start | bytes 24580
  56.6 5.1 %copy-start.12 = (f32[2048]{0:T(1024)S(1)}, f32[2048]{0:T(1024)}, u32[]{:S(2)}) copy-start(f32[2048]{0:T(1024)} %param.35) | copy-start | bytes 24580
  56.6 5.1 %copy-start.13 = (f32[2048]{0:T(1024)S(1)}, f32[2048]{0:T(1024)}, u32[]{:S(2)}) copy-start(f32[2048]{0:T(1024)} %param.41) | copy-start | bytes 24580
  56.9 4.8 %copy-start.1 = (bf16[2048,512]{1,0:T(8,128)(2,1)S(1)}, bf16[2048,512]{1,0:T(8,128)(2,1)}, u32[]{:S(2)}) copy-start(bf16[2048,512]{1,0:T(8,128)(2,1)} %up_hbm.1) | copy-start | bytes 6291460

commit v2 on v1

--- a/solution.py
+++ b/solution.py
@@ -29,25 +29,6 @@
     linear = jnp.clip(upper, -LIMIT, LIMIT)
     return glu * jax.nn.sigmoid(ALPHA * glu) * (linear + 1.0)
 
-
-def delta_step(
-    q_raw, k_raw, v_raw, z_raw, decay_in, beta_in, state, decay_scale, decay_bias, head_gain
-):
-    count = q_raw.shape[0]
-    query = jax.nn.silu(q_raw.astype(jnp.float32)).reshape(count, H, HD)
-    query = query * lax.rsqrt(jnp.sum(query * query, axis=-1, keepdims=True) + EPS) * HD ** (-0.5)
-    keys = jax.nn.silu(k_raw.astype(jnp.float32)).reshape(count, H, HD)
-    keys = keys * lax.rsqrt(jnp.sum(keys * keys, axis=-1, keepdims=True) + EPS)
-    values = jax.nn.silu(v_raw.astype(jnp.float32)).reshape(count, H, HD)
-    decay = -decay_scale * jax.nn.softplus(decay_in + decay_bias)
-    beta = jax.nn.sigmoid(beta_in)
-    held = state.astype(jnp.float32) * jnp.exp(decay)[:, :, None, None]
-    guess = jnp.einsum("rhk,rhkv->rhv", keys, held)
-    held = held + jnp.einsum("rhk,rhv->rhkv", keys, beta[:, :, None] * (values - guess))
-    output = jnp.einsum("rhk,rhkv->rhv", query, held)
-    output = rms_scale(output) * head_gain
-    gated = output.reshape(count, H * HD) * jax.nn.silu(z_raw.astype(jnp.float32))
-    return (gated.astype(jnp.bfloat16), held.astype(jnp.bfloat16))
 
 def flipped(value, distance):
     bit = 1
@@ -85,11 +66,21 @@
         ]
 
 
-def greet(place):
+def greet(partners):
     barrier = pltpu.get_barrier_semaphore()
-    for partner in place.partners():
+    for partner in partners:
         pl.semaphore_signal(barrier, inc=1, device_id=(partner,), device_id_type=MESH)
-    return lambda: pl.semaphore_wait(barrier, len(place.partners()))
+    return lambda: pl.semaphore_wait(barrier, len(partners))
+
+
+def load_all(pairs, sems):
+    loads = [
+        pltpu.make_async_copy(source, target, sems.at[i])
+        for i, (source, target) in enumerate(pairs)
+    ]
+    for load in loads:
+        load.start()
+    return loads
 
 
 def remote(source, target, send_sem, recv_sem, device):
@@ -227,117 +218,289 @@
     )
 
 
+def column_of(row):
+    size = row.shape[1]
+    across = lax.broadcasted_iota(jnp.int32, (size, size), 1)
+    down = lax.broadcasted_iota(jnp.int32, (size, size), 0)
+    return jnp.sum(
+        jnp.where(across == down, jnp.broadcast_to(row, (size, size)), 0.0), axis=1, keepdims=True
+    )
+
+
 def project_kernel(
     devices,
+    own,
+    x_hbm,
+    gain_hbm,
+    routes_hbm,
+    logits_hbm,
+    decay_hbm,
+    beta_hbm,
+    q_hbm,
+    k_hbm,
+    v_hbm,
+    z_hbm,
+    joined,
+    shares_ref,
+    decay_out,
+    beta_out,
     x_ref,
     gain_ref,
     routes_ref,
     logits_ref,
-    q_ref,
-    k_ref,
-    v_ref,
-    z_ref,
     decay_ref,
     beta_ref,
-    columns_ref,
-    shares_ref,
-    decay_out,
-    beta_out,
+    weights,
     buf,
-    weights,
+    columns,
     send_sems,
     recv_sems,
+    out_sems,
+    in_sems,
     load_sems,
 ):
     place = Place(devices)
-    ready = greet(place)
-    width = x_ref.shape[1]
-    own = q_ref.shape[0]
-    loads = [
-        pltpu.make_async_copy(ref, weights.at[pl.ds(i * own, own)], load_sems.at[i])
-        for i, ref in enumerate((q_ref, k_ref, v_ref, z_ref))
-    ]
-    for load in loads:
-        load.start()
+    others = [lax.rem(place.me + i, devices) for i in range(1, devices)]
+    ready = greet(others)
+    count, width = x_ref.shape
+    loads = load_all(
+        [
+            (x_hbm, x_ref),
+            (gain_hbm, gain_ref),
+            (routes_hbm, routes_ref),
+            (logits_hbm, logits_ref),
+            (decay_hbm, decay_ref),
+            (beta_hbm, beta_ref),
+        ]
+        + [
+            (ref, weights.at[pl.ds(i * own, own)])
+            for i, ref in enumerate((q_hbm, k_hbm, v_hbm, z_hbm))
+        ],
+        load_sems,
+    )
+    for load in loads[:4]:
+        load.wait()
     normed = (rms_scale(x_ref[...].astype(jnp.float32)) * gain_ref[...]).astype(jnp.bfloat16)
     raised = jnp.exp(logits_ref[...])
-    shares = raised / jnp.sum(raised, axis=-1, keepdims=True)
-    routes = routes_ref[...]
-    lane = lax.broadcasted_iota(jnp.int32, (x_ref.shape[0], LANES), 1)
+    shares = raised / jnp.sum(raised, axis=0, keepdims=True)
+    routes = routes_ref[...].astype(jnp.float32)
+    lane = lax.broadcasted_iota(jnp.int32, (count, LANES), 1).astype(jnp.float32)
     share = jnp.zeros(lane.shape, jnp.float32)
-    for j in range(routes.shape[1]):
-        share = share + jnp.where(lane == routes[:, j : j + 1], shares[:, j : j + 1], 0.0)
+    for j in range(routes.shape[0]):
+        share = share + jnp.where(
+            lane == column_of(routes[j : j + 1]), column_of(shares[j : j + 1]), 0.0
+        )
     high = share.astype(jnp.bfloat16)
     low = (share - high.astype(jnp.float32)).astype(jnp.bfloat16)
     buf[place.me, :, 0:width] = normed
     buf[place.me, :, width : width + LANES] = high
     buf[place.me, :, width + LANES : width + TAIL] = low
+    ready()
+    started = gather_blocks(place, buf, send_sems, recv_sems)
+    for load in loads[4:]:
+        load.wait()
+    rows = buf[:, :, 0:width].reshape(devices * count, width)
+    columns[...] = dot_t(rows, weights[...]).astype(jnp.bfloat16).reshape(columns.shape)
+    for i, other in enumerate(others):
+        copy = remote(
+            columns.at[other], joined.at[place.me], out_sems.at[i], in_sems.at[place.me], other
+        )
+        copy.start()
+        started.append(copy)
+    joined[place.me] = columns[place.me]
     decay_out[...] = dot_t(normed, decay_ref[...])
     beta_out[...] = dot_t(normed, beta_ref[...])
-    ready()
-    started = gather_blocks(place, buf, send_sems, recv_sems)
-    for load in loads:
-        load.wait()
-    count = x_ref.shape[0]
-    rows = buf[:, :, 0:width].reshape(devices * count, width)
-    columns = dot_t(rows, weights[...])
-    columns_ref[...] = columns.astype(jnp.bfloat16).reshape(columns_ref.shape)
     shares_ref[...] = buf[:, :, width:]
+    for other in others:
+        remote(
+            columns.at[other], joined.at[other], out_sems.at[0], in_sems.at[other], other
+        ).wait_recv()
     settle(started)
 
 
 def project(devices, x, gain, routes, logits, w_query, w_key, w_value, w_outgate, w_decay, w_beta):
     count, width = x.shape
     own = w_query.shape[1]
+    block = max(4 * own, LANES)
     vmem = pl.BlockSpec(memory_space=pltpu.VMEM)
-    hbm = pl.BlockSpec(memory_space=pl.ANY)
+    hbm = pl.BlockSpec(memory_space=pltpu.HBM)
     heads = w_decay.shape[1]
+    dma = pltpu.SemaphoreType.DMA
+    inputs = (
+        x,
+        gain[None],
+        routes.T,
+        logits.T,
+        w_decay.T,
+        w_beta.T,
+        w_query.T,
+        w_key.T,
+        w_value.T,
+        w_outgate.T,
+    )
     return pl.pallas_call(
-        functools.partial(project_kernel, devices),
+        functools.partial(project_kernel, devices, own),
         out_shape=(
-            jax.ShapeDtypeStruct((devices, count, 4 * own), jnp.bfloat16),
+            jax.ShapeDtypeStruct((devices, count, block), jnp.bfloat16),
             jax.ShapeDtypeStruct((devices, count, TAIL), jnp.bfloat16),
             jax.ShapeDtypeStruct((count, heads), jnp.float32),
             jax.ShapeDtypeStruct((count, heads), jnp.float32),
         ),
-        in_specs=[vmem] * 4 + [hbm] * 4 + [vmem] * 2,
+        in_specs=[hbm] * len(inputs),
         out_specs=(vmem,) * 4,
-        scratch_shapes=[
+        scratch_shapes=[pltpu.VMEM(a.shape, a.dtype) for a in inputs[:6]]
+        + [
+            pltpu.VMEM((block, width), jnp.bfloat16),
             pltpu.VMEM((devices, count, width + TAIL), jnp.bfloat16),
-            pltpu.VMEM((4 * own, width), jnp.bfloat16),
-            pltpu.SemaphoreType.DMA((gather_sends(devices),)),
-            pltpu.SemaphoreType.DMA((devices,)),
-            pltpu.SemaphoreType.DMA((4,)),
+            pltpu.VMEM((devices, count, block), jnp.bfloat16),
+            dma((gather_sends(devices),)),
+            dma((devices,)),
+            dma((devices,)),
+            dma((devices,)),
+            dma((len(inputs),)),
         ],
         compiler_params=pltpu.CompilerParams(
-            collective_id=0, has_side_effects=True, vmem_limit_bytes=32 << 20
+            collective_id=0, has_side_effects=True, vmem_limit_bytes=20 << 20
         ),
-    )(
-        x,
-        gain[None],
-        routes,
-        logits,
-        w_query.T,
-        w_key.T,
-        w_value.T,
-        w_outgate.T,
-        w_decay.T,
-        w_beta.T,
-    )
+    )(*inputs)
+
+
+def head_rows(joined, head, kind, own):
+    lane = lax.broadcasted_iota(jnp.int32, (joined.shape[1], LANES), 1)
+    value = jnp.zeros(lane.shape, jnp.float32)
+    group, offset = divmod(kind * own, LANES)
+    for i in range(HD // own):
+        piece = joined[head * (HD // own) + i, :, group * LANES : (group + 1) * LANES]
+        piece = piece.astype(jnp.float32)
+        shift = (i * own - offset) % LANES
+        if shift:
+            piece = pltpu.roll(piece, shift, 1)
+        value = jnp.where((lane >= i * own) & (lane < (i + 1) * own), piece, value)
+    return value
+
+
+def delta_kernel(
+    own,
+    joined,
+    decay_in,
+    beta_in,
+    scale_ref,
+    bias_ref,
+    head_gain_ref,
+    state_hbm,
+    w_out_hbm,
+    branch_ref,
+    new_hbm,
+    state,
+    fresh,
+    w_out,
+    mixed,
+    state_sems,
+    fresh_sems,
+    out_sems,
+):
+    heads = mixed.shape[0]
+    count = state.shape[0]
+    width = w_out.shape[1]
+
+    def state_in(h):
+        return pltpu.make_async_copy(state_hbm.at[:, h], state.at[:, h], state_sems.at[h])
+
+    def state_out(h):
+        return pltpu.make_async_copy(fresh.at[:, h], new_hbm.at[:, h], fresh_sems.at[h])
+
+    for h in range(heads):
+        state_in(h).start()
+    w_load = pltpu.make_async_copy(w_out_hbm, w_out, out_sems.at[0])
+    w_load.start()
+    decay = jnp.exp(-scale_ref[...] * jax.nn.softplus(decay_in[...] + bias_ref[...]))
+    strength = jax.nn.sigmoid(beta_in[...])
+    lane = lax.broadcasted_iota(jnp.int32, decay.shape, 1)
+
+    def one(h, carry):
+        query = jax.nn.silu(head_rows(joined, h, 0, own))
+        query = (
+            query * lax.rsqrt(jnp.sum(query * query, axis=-1, keepdims=True) + EPS) * HD ** (-0.5)
+        )
+        keys = jax.nn.silu(head_rows(joined, h, 1, own))
+        keys = keys * lax.rsqrt(jnp.sum(keys * keys, axis=-1, keepdims=True) + EPS)
+        values = jax.nn.silu(head_rows(joined, h, 2, own))
+        outgate = jax.nn.silu(head_rows(joined, h, 3, own))
+        keep = jnp.sum(jnp.where(lane == h, decay, 0.0), axis=1, keepdims=True)
+        beta = jnp.sum(jnp.where(lane == h, strength, 0.0), axis=1, keepdims=True)
+        overlap = jnp.sum(keys * query, axis=1, keepdims=True)
+        upright = jnp.transpose(jnp.concatenate([keys, query], axis=0))
+        state_in(h).wait()
+        outputs = []
+        for r in range(count):
+            held = state[r, h].astype(jnp.float32)
+            key = jnp.broadcast_to(upright[:, r : r + 1], held.shape)
+            ask = jnp.broadcast_to(upright[:, count + r : count + r + 1], held.shape)
+            rate = keep[r : r + 1]
+            guess = rate * jnp.sum(key * held, axis=0, keepdims=True)
+            change = beta[r : r + 1] * (values[r : r + 1] - guess)
+            seen = rate * jnp.sum(ask * held, axis=0, keepdims=True)
+            outputs.append(seen + overlap[r : r + 1] * change)
+            fresh[r, h] = (rate * held + key * change).astype(jnp.bfloat16)
+        state_out(h).start()
+        output = rms_scale(jnp.concatenate(outputs, axis=0)) * head_gain_ref[...]
+        mixed[h] = (output * outgate).astype(jnp.bfloat16)
+        return carry
+
+    lax.fori_loop(0, heads, one, 0)
+    w_load.wait()
+    rows = jnp.concatenate([mixed[h] for h in range(heads)], axis=1)
+    for j in range(0, width, 512):
+        branch_ref[:, j : j + 512] = jnp.dot(
+            rows, w_out[:, j : j + 512], preferred_element_type=jnp.float32
+        )
+    for h in range(heads):
+        state_out(h).wait()
+
+
+def delta_part(own, joined, decay_in, beta_in, scale, bias, head_gain, state, w_out):
+    count, heads = state.shape[:2]
+    vmem = pl.BlockSpec(memory_space=pltpu.VMEM)
+    hbm = pl.BlockSpec(memory_space=pltpu.HBM)
+    dma = pltpu.SemaphoreType.DMA
+    return pl.pallas_call(
+        functools.partial(delta_kernel, own),
+        out_shape=(
+            jax.ShapeDtypeStruct((count, w_out.shape[1]), jnp.float32),
+            jax.ShapeDtypeStruct(state.shape, state.dtype),
+        ),
+        in_specs=[vmem] * 6 + [hbm] * 2,
+        out_specs=(vmem, hbm),
+        scratch_shapes=[
+            pltpu.VMEM(state.shape, state.dtype),
+            pltpu.VMEM(state.shape, state.dtype),
+            pltpu.VMEM(w_out.shape, w_out.dtype),
+            pltpu.VMEM((heads, count, HD), jnp.bfloat16),
+            dma((heads,)),
+            dma((heads,)),
+            dma((1,)),
+        ],
+        compiler_params=pltpu.CompilerParams(vmem_limit_bytes=40 << 20),
+    )(joined, decay_in, beta_in, scale[None], bias[None], head_gain[None], state, w_out)
 
 
 def expert_kernel(
     devices,
     branch_ref,
+    shares_ref,
+    x_hbm,
+    gain_mix_hbm,
+    gain_pre_hbm,
+    gain_post_hbm,
+    gate_hbm,
+    up_hbm,
+    down_hbm,
+    result_ref,
     x_ref,
     gain_mix_ref,
     gain_pre_ref,
     gain_post_ref,
-    shares_ref,
-    gate_hbm,
-    up_hbm,
-    down_hbm,
-    result_ref,
+    small_sems,
     buf,
     gate,
     up,
@@ -362,13 +525,19 @@
     fourth_recv,
 ):
     place = Place(devices)
-    ready = greet(place)
-    loads = [
-        pltpu.make_async_copy(source, target, load_sems.at[i])
-        for i, (source, target) in enumerate(((gate_hbm, gate), (up_hbm, up), (down_hbm, down)))
-    ]
-    for load in loads:
-        load.start()
+    ready = greet(place.partners())
+    small = load_all(
+        [
+            (x_hbm, x_ref),
+            (gain_mix_hbm, gain_mix_ref),
+            (gain_pre_hbm, gain_pre_ref),
+            (gain_post_hbm, gain_post_ref),
+        ],
+        small_sems,
+    )
+    loads = load_all([(gate_hbm, gate), (up_hbm, up), (down_hbm, down)], load_sems)
+    for load in small:
+        load.wait()
     count, width = x_ref.shape
     pieces = gate.shape[1]
     pairs = devices // 2
@@ -443,7 +612,7 @@
     pairs = devices // 2
     pieces = w_gate.shape[1]
     vmem = pl.BlockSpec(memory_space=pltpu.VMEM)
-    hbm = pl.BlockSpec(memory_space=pl.ANY)
+    hbm = pl.BlockSpec(memory_space=pltpu.HBM)
     dma = pltpu.SemaphoreType.DMA
 
     def blocks(number):
@@ -452,9 +621,14 @@
     return pl.pallas_call(
         functools.partial(expert_kernel, devices),
         out_shape=jax.ShapeDtypeStruct((count, width), jnp.bfloat16),
-        in_specs=[vmem] * 6 + [hbm] * 3,
+        in_specs=[vmem] * 2 + [hbm] * 7,
         out_specs=vmem,
         scratch_shapes=[
+            pltpu.VMEM(x.shape, x.dtype),
+            pltpu.VMEM((1, width), jnp.float32),
+            pltpu.VMEM((1, width), jnp.float32),
+            pltpu.VMEM((1, width), jnp.float32),
+            dma((4,)),
             blocks(devices),
             pltpu.VMEM(w_gate.shape, jnp.bfloat16),
             pltpu.VMEM(w_up.shape, jnp.bfloat16),
@@ -483,11 +657,11 @@
         ),
     )(
         branch,
+        shares,
         x,
         gain_mix[None],
         gain_pre[None],
         gain_post[None],
-        shares,
         w_gate,
         w_up,
         w_down,
@@ -518,7 +692,7 @@
     gain_ffn_post,
 ):
     devices = lax.axis_size("ep")
-    columns, shares, decay_in, beta_in = project(
+    joined, shares, decay_in, beta_in = project(
         devices,
         residual_in,
         gain_mix_pre,
@@ -531,22 +705,17 @@
         w_decay,
         w_beta,
     )
-    count = residual_in.shape[0]
-    joined = lax.all_to_all(columns, "ep", split_axis=0, concat_axis=0, tiled=True)
-    joined = joined.reshape(devices, count, 4, -1).transpose(2, 1, 0, 3).reshape(4, count, H * HD)
-    mixed, new_state = delta_step(
-        joined[0],
-        joined[1],
-        joined[2],
-        joined[3],
+    branch, new_state = delta_part(
+        w_query.shape[1],
+        joined,
         decay_in,
         beta_in,
-        state_cache,
         decay_scale,
         decay_bias,
         head_gain,
-    )
-    branch = jnp.dot(mixed, w_out, preferred_element_type=jnp.float32)
+        state_cache,
+        w_out,
+    )
     result = experts_part(
         devices,
         branch,

time: 93.6 us -> 92.7 us (level)
  Pallas kernels: 50.6 us -> 74.9 us
  matrix products: 12.1 us -> 0 us
  other arithmetic: 8.02 us -> 0 us
  waiting for transfers between devices: 6.87 us -> 0 us
  local copies, waits for them, and re-layouts: 10.1 us -> 16.5 us
  starting transfers between devices: 4.37 us -> 0 us
    pallas_call x1 -> x2, Pallas kernels: 19.9 us -> 41.5 us  [the longest x1 26.6 us: project(): pl.pallas_call(functools.partial(project_kernel, devices, own), out_shape...]
    dot_general x3 -> x0, matrix products: 12.1 us -> none  [the longest x1 4.76 us: shards(): branch = jnp.dot(mixed, w_out, preferred_element_type=jnp.float32)]
    unnamed x35 -> x43, local copies, waits for them, and re-layouts: 9.1 us -> 16.5 us
    all_to_all x1 -> x0, waiting for transfers between devices: 6.87 us -> none  [shards(): lax.all_to_all(columns, 'ep', split_axis=0, concat_axis=0, tiled=True)]
    convert_element_type x2 -> x0, other arithmetic: 6.09 us -> none  [the longest x1 6.04 us: delta_step(): return (gated.astype(jnp.bfloat16), held.astype(jnp.bfloat16))]
    all_to_all x1 -> x0, starting transfers between devices: 4.37 us -> none  [shards(): lax.all_to_all(columns, 'ep', split_axis=0, concat_axis=0, tiled=True)]
    pallas_call x1, Pallas kernels: 30.7 us -> 33.4 us  [experts_part(): pl.pallas_call(functools.partial(expert_kernel, devices), out_shape=jax.S...]
  transfers between devices with their start and end apart: 1 -> 0, of which waited for: 1 -> 0; matrix products, arithmetic and copies ran while one was open for 1% -> 0% of each run, Pallas kernels for 0% -> 0%
where the time goes in v2:
time: 92.7 us; the launch traced here: 92.1 us
  Pallas kernels  74.9 us (81%)
  local copies, waits for them, and re-layouts  16.5 us (18%)
    pallas_call x1, Pallas kernels, experts_part(): pl.pallas_call(functools.partial(expert_kernel, devices), out_shape=jax.S...  33.4 us
    pallas_call x1, Pallas kernels, project(): pl.pallas_call(functools.partial(project_kernel, devices, own), out_shape...  26.6 us
    unnamed x43, local copies, waits for them, and re-layouts  16.5 us
    pallas_call x1, Pallas kernels, delta_part(): pl.pallas_call(functools.partial(delta_kernel, own), out_shape=(jax.Shape...  14.9 us

profile of v2, /device:TPU:0, one launch (start us, length us, event | category | flops | bytes accessed | tf_op | source)
XLA Modules:
  0.0 92.1 jit_solution(11517804489174350766)
XLA Ops:
  0.6 0.0 copy-start.4
  0.6 0.9 %copy-done.4 = bf16[2048,64]{0,1:T(8,128)(2,1)S(1)} copy-done((bf16[2048,64]{0,1:T(8,128)(2,1)S(1)}, bf16[2048,64]{0,1:T(8,128)(2,1)}, u32[]{:S(2)}) %copy-start.4) | copy-done | bytes 262168
  1.6 0.0 copy-start.5
  1.6 0.9 %copy-done.5 = bf16[2048,64]{0,1:T(8,128)(2,1)S(1)} copy-done((bf16[2048,64]{0,1:T(8,128)(2,1)S(1)}, bf16[2048,64]{0,1:T(8,128)(2,1)}, u32[]{:S(2)}) %copy-start.5) | copy-done | bytes 262168
  2.5 0.0 copy-start.6
  2.5 0.9 %copy-done.6 = bf16[2048,64]{0,1:T(8,128)(2,1)S(1)} copy-done((bf16[2048,64]{0,1:T(8,128)(2,1)S(1)}, bf16[2048,64]{0,1:T(8,128)(2,1)}, u32[]{:S(2)}) %copy-start.6) | copy-done | bytes 262168
  3.5 0.0 copy-start.7
  3.5 0.9 %copy-done.7 = bf16[2048,64]{0,1:T(8,128)(2,1)S(1)} copy-done((bf16[2048,64]{0,1:T(8,128)(2,1)S(1)}, bf16[2048,64]{0,1:T(8,128)(2,1)}, u32[]{:S(2)}) %copy-start.7) | copy-done | bytes 262168
  4.4 0.0 copy-start.8
  4.4 0.8 copy-done.8
  5.2 0.0 copy-start.10
  5.2 0.8 copy-done.10
  6.0 0.0 copy-start.11
  6.0 0.8 copy-done.11
  6.9 0.0 copy-start.12
  6.9 0.7 copy-done.12
  7.6 0.0 copy-start.16
  7.6 0.7 copy-done.16
  8.3 0.0 copy-start.17
  8.3 0.7 copy-done.17
  8.9 26.6 %shard_map.212 = (bf16[32,8,256]{2,1,0:T(8,128)(2,1)S(1)}, bf16[32,8,256]{2,1,0:T(8,128)(2,1)S(1)}, f32[8,16]{1,0:T(8,128)S(1)}, f32[8,16]{1,0:T(8,128)S(1)}) custom-call(bf16[8,2048]{1,0:T(8,128)(2,1)S(1)} %copy-done.8, f32[1,2048]{1,0:T(1,128)S(1)} %bitcast.21, s32[4,8]{1,0:T(4,128)S(1)} %bitcast.25, f32[4,8]{1,0:T(4,128)S(1)} %bitcast.26, ...), custom_call_target="tpu_custom_call" | custom-call | tf_op jit(solution)/shard_map/pallas_call | solution.py:341
  35.5 0.0 copy-start
  35.5 3.4 %copy-done = bf16[2048,2048]{1,0:T(8,128)(2,1)S(1)} copy-done((bf16[2048,2048]{1,0:T(8,128)(2,1)S(1)}, bf16[2048,2048]{1,0:T(8,128)(2,1)}, u32[]{:S(2)}) %copy-start) | copy-done | bytes 8388632
  38.9 0.0 copy-start.1
  38.9 2.2 %copy-done.1 = bf16[8,16,128,128]{3,2,1,0:T(8,128)(2,1)S(1)} copy-done((bf16[8,16,128,128]{3,2,1,0:T(8,128)(2,1)S(1)}, bf16[8,16,128,128]{3,2,1,0:T(8,128)(2,1)}, u32[]{:S(2)}) %copy-start.1) | copy-done | bytes 4194328
  41.1 0.0 copy-start.18
  41.1 0.7 copy-done.18
  41.7 0.0 copy-start.19
  41.7 0.7 copy-done.19
  42.4 0.0 copy-start.20
  42.4 0.7 copy-done.20
  43.1 0.0 copy-start.2
  43.1 0.0 copy-start.3
  43.1 0.0 copy-start.9
  43.1 0.0 copy-start.13
  43.1 0.0 copy-start.14
  43.1 0.0 copy-start.15
  43.1 14.9 %shard_map.213 = (f32[8,2048]{1,0:T(8,128)S(1)}, bf16[8,16,128,128]{3,2,1,0:T(8,128)(2,1)}) custom-call(bf16[32,8,256]{2,1,0:T(8,128)(2,1)S(1)} %get-tuple-element.8.joined, f32[8,16]{1,0:T(8,128)S(1)} %get-tuple-element.9.decay_in, f32[8,16]{1,0:T(8,128)S(1)} %get-tuple-element.10.beta_in, f32[1,16]{1,0:T(1,128)S(1)} %bitcast.27, f32[1,16]{1,0:T(1,128)S(1)} %bitcast.28, ...), custom_call_target="tpu_custom_call" | custom-call | tf_op jit(solution)/shard_map/pallas_call | solution.py:466
  58.0 0.0 copy-done.2
  58.1 0.0 copy-done.3
  58.1 0.0 copy-done.9
  58.1 0.0 copy-done.13
  58.1 0.0 copy-done.14
  58.1 0.0 copy-done.15
  58.1 33.4 %shard_map.214 = bf16[8,2048]{1,0:T(8,128)(2,1)S(1)} custom-call(f32[8,2048]{1,0:T(8,128)S(1)} %get-tuple-element.11.branch_ref, bf16[32,8,256]{2,1,0:T(8,128)(2,1)S(1)} %get-tuple-element.12.shares_ref, bf16[8,2048]{1,0:T(8,128)(2,1)S(1)} %copy-done.9, f32[1,2048]{1,0:T(1,128)S(1)} %bitcast.22, f32[1,2048]{1,0:T(1,128)S(1)} %bitcast.23, ...), custom_call_target="tpu_custom_call" | custom-call | tf_op jit(solution)/shard_map/pallas_call | solution.py:621
  91.5 0.6 copy.24
Async XLA Ops:
  0.6 1.0 %copy-start.4 = (bf16[2048,64]{0,1:T(8,128)(2,1)S(1)}, bf16[2048,64]{0,1:T(8,128)(2,1)}, u32[]{:S(2)}) copy-start(bf16[2048,64]{0,1:T(8,128)(2,1)} %param.23) | copy-start | bytes 786436
  1.6 0.9 %copy-start.5 = (bf16[2048,64]{0,1:T(8,128)(2,1)S(1)}, bf16[2048,64]{0,1:T(8,128)(2,1)}, u32[]{:S(2)}) copy-start(bf16[2048,64]{0,1:T(8,128)(2,1)} %param.24) | copy-start | bytes 786436
  2.5 0.9 %copy-start.6 = (bf16[2048,64]{0,1:T(8,128)(2,1)S(1)}, bf16[2048,64]{0,1:T(8,128)(2,1)}, u32[]{:S(2)}) copy-start(bf16[2048,64]{0,1:T(8,128)(2,1)} %param.25) | copy-start | bytes 786436
  3.5 0.9 %copy-start.7 = (bf16[2048,64]{0,1:T(8,128)(2,1)S(1)}, bf16[2048,64]{0,1:T(8,128)(2,1)}, u32[]{:S(2)}) copy-start(bf16[2048,64]{0,1:T(8,128)(2,1)} %param.26) | copy-start | bytes 786436
  4.4 0.8 copy-start.8
  5.2 0.8 copy-start.10
  6.0 0.8 copy-start.11
  6.9 0.7 copy-start.12
  7.6 0.7 copy-start.16
  8.3 0.7 copy-start.17
  35.5 3.4 %copy-start = (bf16[2048,2048]{1,0:T(8,128)(2,1)S(1)}, bf16[2048,2048]{1,0:T(8,128)(2,1)}, u32[]{:S(2)}) copy-start(bf16[2048,2048]{1,0:T(8,128)(2,1)} %w_out_hbm.1) | copy-start | bytes 25165828
  38.9 2.2 %copy-start.1 = (bf16[8,16,128,128]{3,2,1,0:T(8,128)(2,1)S(1)}, bf16[8,16,128,128]{3,2,1,0:T(8,128)(2,1)}, u32[]{:S(2)}) copy-start(bf16[8,16,128,128]{3,2,1,0:T(8,128)(2,1)} %state_hbm.1) | copy-start | bytes 12582916
  41.1 0.7 copy-start.18
  41.7 0.7 copy-start.19
  42.4 0.7 copy-start.20
  43.1 15.0 %copy-start.2 = (bf16[2048,512]{1,0:T(8,128)(2,1)S(1)}, bf16[2048,512]{1,0:T(8,128)(2,1)}, u32[]{:S(2)}) copy-start(bf16[2048,512]{1,0:T(8,128)(2,1)} %gate_hbm.1) | copy-start | bytes 6291460
  43.1 15.0 %copy-start.3 = (bf16[2048,512]{1,0:T(8,128)(2,1)S(1)}, bf16[2048,512]{1,0:T(8,128)(2,1)}, u32[]{:S(2)}) copy-start(bf16[2048,512]{1,0:T(8,128)(2,1)} %up_hbm.1) | copy-start | bytes 6291460
  43.1 15.0 %copy-start.9 = (bf16[8,2048]{1,0:T(8,128)(2,1)S(1)}, bf16[8,2048]{1,0:T(8,128)(2,1)}, u32[]{:S(2)}) copy-start(bf16[8,2048]{1,0:T(8,128)(2,1)} %x_hbm.3) | copy-start | bytes 98308
  43.1 15.0 %copy-start.13 = (f32[2048]{0:T(1024)S(1)}, f32[2048]{0:T(1024)}, u32[]{:S(2)}) copy-start(f32[2048]{0:T(1024)} %param.33) | copy-start | bytes 24580
  43.1 15.0 %copy-start.14 = (f32[2048]{0:T(1024)S(1)}, f32[2048]{0:T(1024)}, u32[]{:S(2)}) copy-start(f32[2048]{0:T(1024)} %param.35) | copy-start | bytes 24580
  43.1 15.0 %copy-start.15 = (f32[2048]{0:T(1024)S(1)}, f32[2048]{0:T(1024)}, u32[]{:S(2)}) copy-start(f32[2048]{0:T(1024)} %param.41) | copy-start | bytes 24580

commit v3 on v2

--- a/solution.py
+++ b/solution.py
@@ -13,6 +13,7 @@
 TOPK = 4
 LANES = 128
 TAIL = 2 * LANES
+VMEM_LIMIT = 66 * 1000 * 1000
 MESH = pl.DeviceIdType.MESH
 
 EPS = 1e-06
@@ -360,7 +361,7 @@
             dma((len(inputs),)),
         ],
         compiler_params=pltpu.CompilerParams(
-            collective_id=0, has_side_effects=True, vmem_limit_bytes=20 << 20
+            collective_id=0, has_side_effects=True, vmem_limit_bytes=VMEM_LIMIT
         ),
     )(*inputs)
 
@@ -480,7 +481,7 @@
             dma((heads,)),
             dma((1,)),
         ],
-        compiler_params=pltpu.CompilerParams(vmem_limit_bytes=40 << 20),
+        compiler_params=pltpu.CompilerParams(vmem_limit_bytes=VMEM_LIMIT),
     )(joined, decay_in, beta_in, scale[None], bias[None], head_gain[None], state, w_out)
 
 
@@ -653,7 +654,7 @@
             dma((layers,)),
         ],
         compiler_params=pltpu.CompilerParams(
-            collective_id=1, has_side_effects=True, vmem_limit_bytes=48 << 20
+            collective_id=1, has_side_effects=True, vmem_limit_bytes=VMEM_LIMIT
         ),
     )(
         branch,

time: 92.7 us -> 81.5 us (0.88)
  local copies, waits for them, and re-layouts: 16.5 us -> 1.38 us
  Pallas kernels: 74.9 us -> 79.3 us
    unnamed x43 -> x1, local copies, waits for them, and re-layouts: 16.5 us -> 1.38 us
    pallas_call x1, Pallas kernels: 33.4 us -> 35.6 us  [experts_part(): pl.pallas_call(functools.partial(expert_kernel, devices), out_shape=jax.S...]
    pallas_call x1, Pallas kernels: 14.9 us -> 16.3 us  [delta_part(): pl.pallas_call(functools.partial(delta_kernel, own), out_shape=(jax.Shape...]
where the time goes in v3:
time: 81.5 us; the launch traced here: 81.3 us
  Pallas kernels  79.3 us (97%)
  local copies, waits for them, and re-layouts  1.38 us (2%)
    pallas_call x1, Pallas kernels, experts_part(): pl.pallas_call(functools.partial(expert_kernel, devices), out_shape=jax.S...  35.6 us
    pallas_call x1, Pallas kernels, project(): pl.pallas_call(functools.partial(project_kernel, devices, own), out_shape...  27.3 us
    pallas_call x1, Pallas kernels, delta_part(): pl.pallas_call(functools.partial(delta_kernel, own), out_shape=(jax.Shape...  16.3 us

profile of v3, /device:TPU:0, one launch (start us, length us, event | category | flops | bytes accessed | tf_op | source)
XLA Modules:
  0.0 81.3 jit_solution(17663811210815289761)
XLA Ops:
  0.6 27.3 %shard_map.212 = (bf16[32,8,256]{2,1,0:T(8,128)(2,1)}, bf16[32,8,256]{2,1,0:T(8,128)(2,1)}, f32[8,16]{1,0:T(8,128)}, f32[8,16]{1,0:T(8,128)}) custom-call(bf16[8,2048]{1,0:T(8,128)(2,1)} %x_hbm.3, f32[1,2048]{1,0:T(1,128)} %bitcast.21, s32[4,8]{1,0:T(4,128)} %bitcast.25, f32[4,8]{1,0:T(4,128)} %bitcast.26, bf16[16,2048]{1,0:T(8,128)(2,1)} %bitcast.19, ...), custom_call_target="tpu_custom_call" | custom-call | tf_op jit(solution)/shard_map/pallas_call | solution.py:342
  28.0 16.3 %shard_map.213 = (f32[8,2048]{1,0:T(8,128)}, bf16[8,16,128,128]{3,2,1,0:T(8,128)(2,1)}) custom-call(bf16[32,8,256]{2,1,0:T(8,128)(2,1)} %get-tuple-element.8.joined, f32[8,16]{1,0:T(8,128)} %get-tuple-element.9.decay_in, f32[8,16]{1,0:T(8,128)} %get-tuple-element.10.beta_in, f32[1,16]{1,0:T(1,128)} %bitcast.27, f32[1,16]{1,0:T(1,128)} %bitcast.28, ...), custom_call_target="tpu_custom_call" | custom-call | tf_op jit(solution)/shard_map/pallas_call | solution.py:467
  44.3 35.6 %shard_map.214 = bf16[8,2048]{1,0:T(8,128)(2,1)} custom-call(f32[8,2048]{1,0:T(8,128)} %get-tuple-element.11.branch_ref, bf16[32,8,256]{2,1,0:T(8,128)(2,1)} %get-tuple-element.12.shares_ref, bf16[8,2048]{1,0:T(8,128)(2,1)} %x_hbm.3, f32[1,2048]{1,0:T(1,128)} %bitcast.22, f32[1,2048]{1,0:T(1,128)} %bitcast.23, f32[1,2048]{1,0:T(1,128)} %bitcast.24, ...), custom_call_target="tpu_custom_call" | custom-call | tf_op jit(solution)/shard_map/pallas_call | solution.py:622
  79.9 1.4 %copy.24 = bf16[8,2048]{1,0:T(8,128)(2,1)} copy(bf16[8,2048]{1,0:T(8,128)(2,1)} %shard_map.214) | data formatting | bytes 65536
